TPU v7x, 1024 devices: a whole 8x8x8 slice. The times are simulated.
1024 devices in a mesh: fs: 64 (over z, y), tp: 16 (over x, core).
Axes of the slice: x: 8, y: 8, z: 8, core: 2. Of those that a mesh axis runs over, the one named last changes fastest.
Arguments:
- tokens: bfloat16 [24576, 2048], P('fs'), may hold values from -6 to 6
- norm_gain: float32 [2048], replicated, may hold values from 0.1 to 1.9
- w_gate: bfloat16 [2048, 4096], P('fs', 'tp'), may hold values from -0.125 to 0.125
- w_up: bfloat16 [2048, 4096], P('fs', 'tp'), may hold values from -0.125 to 0.125
- w_down: bfloat16 [4096, 2048], P('tp', 'fs'), may hold values from -0.09375 to 0.09375
- cotangent: bfloat16 [24576, 2048], P('fs'), may hold values from -16 to 16
Outputs:
- grad_tokens: bfloat16 [24576, 2048], P('fs')
- grad_down: float32 [4096, 2048], P('tp', 'fs')
- down_norms: float32 [4096], P('tp')
All inputs are finite; a program needn't handle non-finite values.
Results may differ from a plain program's by a relative error of at most 0.018.
Values may be sent and summed in bfloat16 or wider, within the bound.
No kernel may reach another device: no remote copies, remote signals or barrier semaphores. Data moves between devices by JAX's collectives and lax.ppermute only.
A program may use at most 32 MiB of HBM per device.

v0:
```python
import functools

import jax
import jax.numpy as jnp
from jax import lax
from jax.sharding import Mesh
from jax.sharding import PartitionSpec as P

FS = ("fs_0", "fs_1")


EPS = 1e-06


def side_by_side(arrays, axis, dim, along):
    widths = [a.shape[along] for a in arrays]
    both = jnp.concatenate(arrays, axis=along)
    out = lax.all_gather(both, axis, axis=dim, tiled=True)
    return tuple(jnp.split(out, [sum(widths[:k]) for k in range(1, len(widths))], axis=along))


def copy_for_each(shard, axis):
    copies = jnp.broadcast_to(shard, (lax.axis_size(axis), *shard.shape))
    return lax.all_to_all(copies, axis, split_axis=0, concat_axis=0, tiled=True)


def in_order(pieces, dim):
    dims = list(pieces.shape[1:])
    dims[dim] *= pieces.shape[0]
    return jnp.moveaxis(pieces, 0, dim).reshape(dims)


def collect(shard, axis, dim):
    pieces = copy_for_each(shard, axis)
    return in_order(pieces, dim)


def own_rows(so_far, axes):
    for axis in axes:
        so_far = lax.psum_scatter(so_far, axis, scatter_dimension=0, tiled=True)
    return so_far


def by_axis(shard, axes):
    return functools.reduce(lax.psum, axes, shard)


def in_blocks(shard, dim, peers):
    dims = shard.shape
    pieces = shard.reshape(*dims[:dim], peers, dims[dim] // peers, *dims[dim + 1 :])
    return jnp.moveaxis(pieces, dim, 0)


def sum_at_owner(shard, axis, dim):
    peers = lax.axis_size(axis)
    pieces = lax.all_to_all(in_blocks(shard, dim, peers), axis, 0, 0, tiled=True)
    return jnp.sum(pieces.astype(jnp.float32), axis=0)


def shards(tokens, norm_gain, w_gate, w_up, w_down, cotangent):
    xf = tokens.astype(jnp.float32)
    inv = lax.rsqrt(jnp.mean(xf * xf, axis=-1, keepdims=True) + EPS)
    scaled = xf * inv
    normed = (scaled * norm_gain).astype(jnp.bfloat16)
    full_gate, full_up = side_by_side((w_gate, w_up), FS, 0, 1)
    gate = jnp.dot(normed, full_gate, preferred_element_type=jnp.float32)
    up = jnp.dot(normed, full_up, preferred_element_type=jnp.float32)
    full_down = collect(w_down, FS, 1)
    d_hidden = 0.5 * lax.dot_general(
        cotangent, full_down, (((1,), (1,)), ((), ())), preferred_element_type=jnp.float32
    )
    sig = jax.nn.sigmoid(gate)
    act = gate * sig
    hidden = (act * up).astype(jnp.bfloat16)
    share = own_rows(
        0.5
        * lax.dot_general(
            cotangent, hidden, (((0,), (0,)), ((), ())), preferred_element_type=jnp.float32
        ),
        FS,
    )
    grad_down = share.T
    down_norms = by_axis(jnp.sum(share * share, axis=0), FS)
    d_gate = (d_hidden * up * sig * (1.0 + gate * (1.0 - sig))).astype(jnp.bfloat16)
    d_up = (d_hidden * act).astype(jnp.bfloat16)
    part = lax.dot_general(
        d_gate, full_gate, (((1,), (1,)), ((), ())), preferred_element_type=jnp.float32
    )
    part = part + lax.dot_general(
        d_up, full_up, (((1,), (1,)), ((), ())), preferred_element_type=jnp.float32
    )
    d_share = sum_at_owner(part.astype(jnp.bfloat16), "tp", 0)
    share_rows = d_share.shape[0]
    offset = lax.axis_index("tp") * share_rows
    scaled_rows = lax.dynamic_slice_in_dim(scaled, offset, share_rows, 0)
    inv_rows = lax.dynamic_slice_in_dim(inv, offset, share_rows, 0)
    d_scaled = d_share * norm_gain
    inner = jnp.mean(d_scaled * scaled_rows, axis=-1, keepdims=True)
    grad_share = (inv_rows * (d_scaled - scaled_rows * inner)).astype(jnp.bfloat16)
    grad_tokens = collect(grad_share, "tp", 0)
    return (grad_tokens, grad_down, down_norms)


def solution(mesh):
    split = Mesh(mesh.devices.reshape(8, 8, mesh.shape["tp"]), ("fs_0", "fs_1", "tp"))
    placed = (P(FS, None), P(), P(FS, "tp"), P(FS, "tp"), P("tp", FS), P(FS, None))
    return jax.shard_map(
        shards,
        mesh=split,
        in_specs=placed,
        out_specs=(P(FS, None), P("tp", FS), P("tp")),
        check_vma=False,
    )
```

profile of v0, /device:TPU:2, one launch (start us, length us, event | category | flops | bytes accessed | tf_op | source)
XLA Modules:
  0.0 274.0 jit_solution(7005611323103751585)
XLA Ops:
  7.2 0.0 copy-start
  7.2 0.0 copy-start.1
  7.2 0.0 all-gather.2.cloned.1.call-start
  7.2 1.5 pad_maximum_fusion
  8.7 0.0 all-gather.2.cloned.1.call-update
  8.8 1.8 broadcast_in_dim.4
  10.6 23.7 %all-to-all-start = ((bf16[64,256,32]{1,2,0:T(8,128)(2,1)}), bf16[64,256,32]{1,2,0:T(8,128)(2,1)}, u32[]{:S(2)}, u32[]{:S(2)}) async-start(bf16[64,256,32]{1,2,0:T(8,128)(2,1)} %broadcast_in_dim.4), calls=%async_computation | async-start | bytes 2097152 | tf_op jit(solution)/shard_map/all_to_all | solution.py:24
  34.3 0.0 copy-done.1
  34.3 0.4 fusion
  34.7 0.0 copy-start.5
  34.7 29.6 %all-to-all-done = bf16[64,256,32]{1,2,0:T(8,128)(2,1)} async-done(((bf16[64,256,32]{1,2,0:T(8,128)(2,1)}), bf16[64,256,32]{1,2,0:T(8,128)(2,1)}, u32[]{:S(2)}, u32[]{:S(2)}) %all-to-all-start) | async-done | bytes 1048608 | tf_op jit(solution)/shard_map/all_to_all | solution.py:24
  64.3 0.0 copy-done
  64.3 2.5 convolution_multiply_fusion.1
  66.8 55.6 %all-gather.2.cloned.1.call-done = bf16[2048,512]{1,0:T(8,128)(2,1)} async-done(((bf16[32,512]{1,0:T(8,128)(2,1)}), bf16[2048,512]{1,0:T(8,128)(2,1)}) %all-gather.2.cloned.1.call-update) | async-done | bytes 2097168 | tf_op jit(solution)/shard_map/all_gather | solution.py:18
  122.4 0.0 copy-done.5
  122.4 0.0 copy-start.2
  122.4 2.0 fusion.4
  124.4 0.0 copy-done.2
  124.5 0.0 copy-start.4
  124.5 0.6 fusion.7
  125.1 0.0 copy-start.3
  125.1 0.7 copy-done.3
  125.8 0.0 copy-done.4
  125.8 0.7 fusion.2
  126.5 1.8 add_convert_fusion
  128.3 7.2 %all-to-all-start.1 = ((bf16[16,24,2048]{2,1,0:T(8,128)(2,1)}), bf16[16,24,2048]{2,1,0:T(8,128)(2,1)S(1)}, u32[]{:S(2)}, u32[]{:S(2)}) async-start(bf16[16,24,2048]{2,1,0:T(8,128)(2,1)} %bitcast.14), calls=%async_computation.1 | async-start | bytes 3145728 | tf_op jit(solution)/shard_map/all_to_all | solution.py:56
  135.6 0.0 reduce-scatter.5.cloned.1.call-start
  135.6 3.1 %fusion.1 = f32[2048,256]{0,1:T(8,128)} fusion(bf16[384,2048]{1,0:T(8,128)(2,1)S(1)} %copy-done, f32[384,256]{1,0:T(8,128)} %copy-done.3, f32[384,256]{1,0:T(8,128)S(1)} %fusion.4), kind=kOutput, calls=%fused_computation.7 | convolution fusion | flops 403767296 | bytes 4456448 | tf_op jit(solution)/shard_map/dot_general | solution.py:77
  138.7 0.0 reduce-scatter.5.cloned.1.call-update
  138.8 0.1 dynamic-slice.3
  138.8 3.3 %convert_multiply_fusion = f32[384,2048]{1,0:T(8,128)} fusion(bf16[384,2048]{1,0:T(8,128)(2,1)} %param.6, f32[384]{0:T(512)S(1)} %add_rsqrt_fusion), kind=kLoop, calls=%fused_computation | loop fusion | flops 1572864 | bytes 4720128 | tf_op jit(solution)/shard_map/mul | solution.py:63
  142.2 29.2 %all-to-all-done.1 = bf16[16,24,2048]{2,1,0:T(8,128)(2,1)S(1)} async-done(((bf16[16,24,2048]{2,1,0:T(8,128)(2,1)}), bf16[16,24,2048]{2,1,0:T(8,128)(2,1)S(1)}, u32[]{:S(2)}, u32[]{:S(2)}) %all-to-all-start.1) | async-done | bytes 1572896 | tf_op jit(solution)/shard_map/all_to_all | solution.py:56
  171.4 0.3 convert_reduce_fusion
  171.7 1.1 multiply_reduce_fusion
  172.7 1.0 multiply_convert_fusion.9
  173.8 1.3 broadcast_in_dim.5
  175.1 6.8 %all-to-all-start.2 = ((bf16[16,24,2048]{2,1,0:T(8,128)(2,1)}), bf16[16,24,2048]{2,1,0:T(8,128)(2,1)S(1)}, u32[]{:S(2)}, u32[]{:S(2)}) async-start(bf16[16,24,2048]{2,1,0:T(8,128)(2,1)} %broadcast_in_dim.5), calls=%async_computation.2 | async-start | bytes 3145728 | tf_op jit(solution)/shard_map/all_to_all | solution.py:24
  181.9 0.0 reduce-scatter.7.cloned.1.call-start
  182.0 3.9 %reduce-scatter.5.cloned.1.call-done = f32[256,256]{0,1:T(8,128)} async-done(((f32[2048,256]{0,1:T(8,128)}), f32[256,256]{0,1:T(8,128)}) %reduce-scatter.5.cloned.1.call-update) | async-done | bytes 262160 | tf_op jit(solution)/shard_map/reduce_scatter | solution.py:40
  185.9 1.8 copy.13
  187.6 0.0 reduce-scatter.7.cloned.1.call-update
  187.7 42.1 %reduce-scatter.7.cloned.1.call-done = f32[32,256]{1,0:T(8,128)} async-done(((f32[256,256]{1,0:T(8,128)}), f32[32,256]{1,0:T(8,128)}) %reduce-scatter.7.cloned.1.call-update) | async-done | bytes 32784
  229.8 0.9 copy.14
  230.6 0.1 multiply_reduce_fusion.1
  230.8 19.4 %psum.14 = f32[256]{0:T(256)S(1)} all-reduce(f32[256]{0:T(256)S(1)} %multiply_reduce_fusion.1), channel_id=1, replica_groups=mesh['fs_0'=8,'fs_1'=8,'tp'=16] {'fs_0'}, use_global_device_ids=true, to_apply=%region_6.0 | all-reduce | flops 256 | bytes 2048 | tf_op jit(solution)/shard_map/psum | solution.py:45
  250.1 16.1 %psum.15 = f32[256]{0:T(256)} all-reduce(f32[256]{0:T(256)S(1)} %psum.14), channel_id=1, replica_groups=mesh['fs_0'=8,'fs_1'=8,'tp'=16] {'fs_1'}, use_global_device_ids=true, to_apply=%region_7.0 | all-reduce | flops 256 | bytes 2048 | tf_op jit(solution)/shard_map/psum | solution.py:45
  266.3 0.0 all-to-all-done.2
  266.3 1.1 copy.17
  (2 shorter events, 0.0 us)
Async XLA Ops:
  7.2 57.1 %copy-start = (bf16[384,2048]{1,0:T(8,128)(2,1)S(1)}, bf16[384,2048]{1,0:T(8,128)(2,1)}, u32[]{:S(2)}) copy-start(bf16[384,2048]{1,0:T(8,128)(2,1)} %param.11) | copy-start | bytes 4718596
  7.2 27.1 %copy-start.1 = (bf16[384,2048]{1,0:T(8,128)(2,1)S(1)}, bf16[384,2048]{1,0:T(8,128)(2,1)}, u32[]{:S(2)}) copy-start(bf16[384,2048]{1,0:T(8,128)(2,1)} %param.6) | copy-start | bytes 4718596
  7.2 115.2 %all-gather.2.cloned.1.call-start = ((), (), s32[]{:S(2)}) async-start(), calls=%async_computation.5 | async-start | bytes 2129920 | tf_op jit(solution)/shard_map/all_gather | solution.py:18
  10.6 53.7 %all-to-all-start = ((bf16[64,256,32]{1,2,0:T(8,128)(2,1)}), bf16[64,256,32]{1,2,0:T(8,128)(2,1)}, u32[]{:S(2)}, u32[]{:S(2)}) async-start(bf16[64,256,32]{1,2,0:T(8,128)(2,1)} %broadcast_in_dim.4), calls=%async_computation | async-start | bytes 2097152 | tf_op jit(solution)/shard_map/all_to_all | solution.py:24
  34.7 87.8 %copy-start.5 = (f32[2048]{0:T(1024)S(1)}, f32[2048]{0:T(1024)}, u32[]{:S(2)}) copy-start(f32[2048]{0:T(1024)} %param.7) | copy-start | bytes 24580
  122.4 2.0 copy-start.2
  124.5 1.4 copy-start.4
  125.1 0.7 copy-start.3
  128.3 43.1 %all-to-all-start.1 = ((bf16[16,24,2048]{2,1,0:T(8,128)(2,1)}), bf16[16,24,2048]{2,1,0:T(8,128)(2,1)S(1)}, u32[]{:S(2)}, u32[]{:S(2)}) async-start(bf16[16,24,2048]{2,1,0:T(8,128)(2,1)} %bitcast.14), calls=%async_computation.1 | async-start | bytes 3145728 | tf_op jit(solution)/shard_map/all_to_all | solution.py:56
  135.6 50.3 %reduce-scatter.5.cloned.1.call-start = ((), (), s32[]{:S(2)}) async-start(), calls=%async_computation.6 | async-start | bytes 2359296 | tf_op jit(solution)/shard_map/reduce_scatter | solution.py:40
  175.1 91.2 %all-to-all-start.2 = ((bf16[16,24,2048]{2,1,0:T(8,128)(2,1)}), bf16[16,24,2048]{2,1,0:T(8,128)(2,1)S(1)}, u32[]{:S(2)}, u32[]{:S(2)}) async-start(bf16[16,24,2048]{2,1,0:T(8,128)(2,1)} %broadcast_in_dim.5), calls=%async_computation.2 | async-start | bytes 3145728 | tf_op jit(solution)/shard_map/all_to_all | solution.py:24
  181.9 47.9 %reduce-scatter.7.cloned.1.call-start = ((), (), s32[]{:S(2)}) async-start(), calls=%async_computation.7 | async-start | bytes 294912
Sparse Core Ops, SparseCore 0:
  12.8 109.5 all-gather.1
  139.8 46.0 reduce-scatter.4
  189.8 39.9 reduce-scatter.6
where the time goes:
time: 275 us; the launch traced here: 274 us
  waiting for transfers between devices  161 us (59%)
  starting transfers between devices  37.8 us (14%)
  blocking collectives  35.5 us (13%)
  between operations  13.9 us (5%)
  matrix products  10.8 us (4%)
  local copies, waits for them, and re-layouts  7.75 us (3%)
  other arithmetic  7.71 us (3%)
    all_gather x1, waiting for transfers between devices, side_by_side(): out = lax.all_gather(both, axis, axis=dim, tiled=True)  55.6 us
    unnamed x4, waiting for transfers between devices  42.2 us
    psum x2, blocking collectives, by_axis(): return functools.reduce(lax.psum, axes, shard)  35.5 us
    all_to_all x2, starting transfers between devices, copy_for_each(): return lax.all_to_all(copies, axis, split_axis=0, concat_axis=0, tiled=True)  30.5 us
    all_to_all x2, waiting for transfers between devices, copy_for_each(): return lax.all_to_all(copies, axis, split_axis=0, concat_axis=0, tiled=True)  29.6 us
    all_to_all x1, waiting for transfers between devices, sum_at_owner(): lax.all_to_all(in_blocks(shard, dim, peers), axis, 0, 0, tiled=True)  29.2 us
    all_to_all x1, starting transfers between devices, sum_at_owner(): lax.all_to_all(in_blocks(shard, dim, peers), axis, 0, 0, tiled=True)  7.24 us
  transfers between devices with their start and end apart: 6, of which 5 were waited for; matrix products, arithmetic and copies ran while one was open for 6% of the time, Pallas kernels for 0%

commit v1 on v0

v1 whole, which is shorter than its diff:
```python
import jax
import jax.numpy as jnp
from jax import lax
from jax.sharding import Mesh
from jax.sharding import PartitionSpec as P

FS = ("z", "y")
TP = ("x", "c")


EPS = 1e-06


def swap(pieces, axis):
    return lax.all_to_all(pieces, axis, split_axis=0, concat_axis=0, tiled=True)


def copy_for_each(shard, axis):
    return swap(jnp.broadcast_to(shard, (lax.axis_size(axis), *shard.shape)), axis)


def shards(tokens, norm_gain, w_gate, w_up, w_down, cotangent):
    f32, bf16 = jnp.float32, jnp.bfloat16
    rows, width = tokens.shape
    part_rows, units = w_gate.shape
    half = units // 2
    sizes = {a: lax.axis_size(a) for a in ("z", "y", "x", "c")}

    down_t = w_down.T
    first = jnp.concatenate([w_gate, down_t[:, :half]], axis=1)
    second = jnp.concatenate([w_up, down_t[:, half:]], axis=1)
    first = copy_for_each(first, "y")
    second = copy_for_each(second, "z")
    first = copy_for_each(first, "z")
    second = copy_for_each(second, "y")
    first = first.reshape(width, -1)
    second = jnp.swapaxes(second, 0, 1).reshape(width, -1)
    full_gate, down_a = first[:, :units], first[:, units:]
    full_up, down_b = second[:, :units], second[:, units:]

    xf = tokens.astype(f32)
    inv = lax.rsqrt(jnp.mean(xf * xf, axis=-1, keepdims=True) + EPS)
    normed = (xf * inv * norm_gain).astype(bf16)
    gate = jnp.dot(normed, full_gate, preferred_element_type=f32)
    up = jnp.dot(normed, full_up, preferred_element_type=f32)
    d_hidden = 0.5 * jnp.concatenate(
        [jnp.dot(cotangent, w, preferred_element_type=f32) for w in (down_a, down_b)], axis=1
    )
    sig = jax.nn.sigmoid(gate)
    act = gate * sig
    hidden = (act * up).astype(bf16)
    d_gate = (d_hidden * up * sig * (1.0 + gate * (1.0 - sig))).astype(bf16)
    d_up = (d_hidden * act).astype(bf16)

    part = lax.dot_general(d_gate, full_gate, (((1,), (1,)), ((), ())), preferred_element_type=f32)
    part = part + lax.dot_general(
        d_up, full_up, (((1,), (1,)), ((), ())), preferred_element_type=f32
    )
    pair = swap(part.astype(bf16).reshape(sizes["c"], rows // sizes["c"], width), "c")
    mine = jnp.sum(pair.astype(f32), axis=0).astype(bf16)
    own = mine.shape[0] // sizes["x"]
    pieces = swap(mine.reshape(sizes["x"], own, width), "x")

    down_part = 0.5 * lax.dot_general(
        cotangent, hidden, (((0,), (0,)), ((), ())), preferred_element_type=f32
    )
    down_pieces = swap(down_part.astype(bf16).reshape(-1, part_rows, units), FS)
    share = jnp.sum(down_pieces.astype(f32), axis=0)
    norms = copy_for_each(jnp.sum(share * share, axis=0), FS)

    d_share = jnp.sum(pieces.astype(f32), axis=0)
    offset = (lax.axis_index("c") * sizes["x"] + lax.axis_index("x")) * own
    own_tokens = lax.dynamic_slice_in_dim(tokens, offset, own, 0).astype(f32)
    own_inv = lax.rsqrt(jnp.mean(own_tokens * own_tokens, axis=-1, keepdims=True) + EPS)
    scaled = own_tokens * own_inv
    d_scaled = d_share * norm_gain
    inner = jnp.mean(d_scaled * scaled, axis=-1, keepdims=True)
    grad_own = (own_inv * (d_scaled - scaled * inner)).astype(bf16)
    grad_half = copy_for_each(grad_own, "x").reshape(-1, width)
    grad_tokens = copy_for_each(grad_half, "c").reshape(rows, width)
    return (grad_tokens, share.T, jnp.sum(norms, axis=0))


def solution(mesh):
    split = Mesh(mesh.devices.reshape(8, 8, 8, 2), ("z", "y", "x", "c"))
    placed = (P(FS, None), P(), P(FS, TP), P(FS, TP), P(TP, FS), P(FS, None))
    return jax.shard_map(
        shards,
        mesh=split,
        in_specs=placed,
        out_specs=(P(FS, None), P(TP, FS), P(TP)),
        check_vma=False,
    )
```

time: 275 us -> 260 us (0.945)
  the two profiles are of different devices: /device:TPU:2 before, /device:TPU:1 now
where the time goes in v1:
time: 260 us; the launch traced here: 259 us
  waiting for transfers between devices  116 us (45%)
  blocking collectives  80.3 us (31%)
  starting transfers between devices  34.5 us (13%)
  local copies, waits for them, and re-layouts  10.6 us (4%)
  other arithmetic  9.09 us (3%)
  matrix products  7.54 us (3%)
    all_to_all x6, waiting for transfers between devices, swap(): return lax.all_to_all(pieces, axis, split_axis=0, concat_axis=0, tiled=True)  116 us
    all_to_all x4, blocking collectives, swap(): return lax.all_to_all(pieces, axis, split_axis=0, concat_axis=0, tiled=True)  80.3 us
    all_to_all x6, starting transfers between devices, swap(): return lax.all_to_all(pieces, axis, split_axis=0, concat_axis=0, tiled=True)  34.5 us
  transfers between devices with their start and end apart: 6, of which 6 were waited for; matrix products, arithmetic and copies ran while one was open for 5% of the time, Pallas kernels for 0%

profile of v1, /device:TPU:1, one launch (start us, length us, event | category | flops | bytes accessed | tf_op | source)
XLA Modules:
  0.0 259.2 jit_solution(9308528906519789420)
XLA Ops:
  0.6 0.0 copy-start
  0.6 0.8 fusion.36
  1.5 0.7 pad_maximum_fusion
  2.2 0.7 broadcast_in_dim.26
  2.9 8.1 %all-to-all-start = ((bf16[8,32,384]{2,1,0:T(8,128)(2,1)}), bf16[8,32,384]{2,1,0:T(8,128)(2,1)S(1)}, u32[]{:S(2)}, u32[]{:S(2)}) async-start(bf16[8,32,384]{2,1,0:T(8,128)(2,1)} %broadcast_in_dim.26), calls=%async_computation | async-start | bytes 393216 | tf_op jit(solution)/shard_map/all_to_all | solution.py:15
  11.0 0.7 pad_maximum_fusion.1
  11.7 7.9 %all-to-all-done = bf16[8,32,384]{2,1,0:T(8,128)(2,1)S(1)} async-done(((bf16[8,32,384]{2,1,0:T(8,128)(2,1)}), bf16[8,32,384]{2,1,0:T(8,128)(2,1)S(1)}, u32[]{:S(2)}, u32[]{:S(2)}) %all-to-all-start) | async-done | bytes 196640 | tf_op jit(solution)/shard_map/all_to_all | solution.py:15
  19.6 25.5 %all_to_all.51 = bf16[8,32,384]{2,1,0:T(8,128)(2,1)S(1)} all-to-all(bf16[8,32,384]{2,1,0:T(8,128)(2,1)S(1)} %broadcast_in_dim.28), channel_id=1, replica_groups=mesh['z'=8,'y'=8,'x'=8,'c'=2] {'z'}, dimensions={0} | all-to-all | bytes 393216 | tf_op jit(solution)/shard_map/all_to_all | solution.py:15
  45.1 0.2 broadcast_in_dim.27
  45.3 38.6 %all_to_all.52 = bf16[8,8,32,384]{3,2,1,0:T(8,128)(2,1)} all-to-all(bf16[8,8,32,384]{3,2,1,0:T(8,128)(2,1)S(1)} %broadcast_in_dim.27), channel_id=1, replica_groups=mesh['z'=8,'y'=8,'x'=8,'c'=2] {'z'}, dimensions={0} | all-to-all | bytes 3145728 | tf_op jit(solution)/shard_map/all_to_all | solution.py:15
  83.9 1.3 broadcast_in_dim.29
  85.2 0.0 copy-start.8
  85.2 4.1 %all-to-all-start.3 = ((bf16[8,8,32,384]{3,2,1,0:T(8,128)(2,1)}), bf16[8,8,32,384]{3,2,1,0:T(8,128)(2,1)S(1)}, u32[]{:S(2)}, u32[]{:S(2)}) async-start(bf16[8,8,32,384]{3,2,1,0:T(8,128)(2,1)} %broadcast_in_dim.29), calls=%async_computation.3 | async-start | bytes 3145728 | tf_op jit(solution)/shard_map/all_to_all | solution.py:15
  89.4 0.0 copy-start.1
  89.4 1.9 fusion
  91.3 0.0 copy-done.8
  91.3 0.0 copy-done.1
  91.3 2.3 fusion.7
  93.6 33.0 %all-to-all-done.3 = bf16[8,8,32,384]{3,2,1,0:T(8,128)(2,1)S(1)} async-done(((bf16[8,8,32,384]{3,2,1,0:T(8,128)(2,1)}), bf16[8,8,32,384]{3,2,1,0:T(8,128)(2,1)S(1)}, u32[]{:S(2)}, u32[]{:S(2)}) %all-to-all-start.3) | async-done | bytes 1572896 | tf_op jit(solution)/shard_map/all_to_all | solution.py:15
  126.6 0.0 copy-start.3
  126.6 0.2 copy.34
  126.8 1.2 copy-done.3
  128.0 0.9 fusion.10
  128.9 0.0 copy-done
  128.9 0.0 copy-start.5
  128.9 0.0 copy-start.2
  128.9 0.6 convolution_bitcast_fusion
  129.6 0.9 copy-done.2
  130.5 0.6 convolution_bitcast_fusion.1
  131.1 0.0 copy-done.5
  131.1 0.7 fusion.5
  131.8 0.7 add_convert_fusion
  132.5 8.4 %all_to_all.53 = bf16[2,192,2048]{2,1,0:T(8,128)(2,1)S(1)} all-to-all(bf16[2,192,2048]{2,1,0:T(8,128)(2,1)S(1)} %bitcast.24), channel_id=1, replica_groups=mesh['z'=8,'y'=8,'x'=8,'c'=2] {'c'}, dimensions={0} | all-to-all | bytes 3145728 | tf_op jit(solution)/shard_map/all_to_all | solution.py:15
  140.9 1.4 reduce_sum.77
  142.3 0.0 copy-start.6
  142.3 6.6 %all-to-all-start.5 = ((bf16[8,24,2048]{2,1,0:T(8,128)(2,1)}), bf16[8,24,2048]{2,1,0:T(8,128)(2,1)S(1)}, u32[]{:S(2)}, u32[]{:S(2)}) async-start(bf16[8,24,2048]{2,1,0:T(8,128)(2,1)} %bitcast.28), calls=%async_computation.5 | async-start | bytes 1572864 | tf_op jit(solution)/shard_map/all_to_all | solution.py:15
  148.9 0.0 copy-done.6
  148.9 1.7 fusion.4
  150.6 2.3 copy.40
  152.9 19.6 %all-to-all-done.5 = bf16[8,24,2048]{2,1,0:T(8,128)(2,1)S(1)} async-done(((bf16[8,24,2048]{2,1,0:T(8,128)(2,1)}), bf16[8,24,2048]{2,1,0:T(8,128)(2,1)S(1)}, u32[]{:S(2)}, u32[]{:S(2)}) %all-to-all-start.5) | async-done | bytes 786464 | tf_op jit(solution)/shard_map/all_to_all | solution.py:15
  172.5 4.7 %all-to-all-start.8 = ((bf16[64,32,256]{2,1,0:T(8,128)(2,1)}), bf16[64,32,256]{2,1,0:T(8,128)(2,1)S(1)}, u32[]{:S(2)}, u32[]{:S(2)}) async-start(bf16[64,32,256]{2,1,0:T(8,128)(2,1)} %bitcast.12), calls=%async_computation.8 | async-start | bytes 2097152 | tf_op jit(solution)/shard_map/all_to_all | solution.py:15
  177.2 1.0 fusion.23
  178.2 0.1 convert_reduce_fusion.1
  178.3 0.0 copy-start.4
  178.3 1.2 fusion.19
  179.5 0.0 copy-done.4
  179.5 25.8 %all-to-all-done.8 = bf16[64,32,256]{2,1,0:T(8,128)(2,1)S(1)} async-done(((bf16[64,32,256]{2,1,0:T(8,128)(2,1)}), bf16[64,32,256]{2,1,0:T(8,128)(2,1)S(1)}, u32[]{:S(2)}, u32[]{:S(2)}) %all-to-all-start.8) | async-done | bytes 1048608 | tf_op jit(solution)/shard_map/all_to_all | solution.py:15
  205.3 0.2 convert_reduce_fusion
  205.5 0.0 copy-start.7
  205.5 0.7 broadcast_in_dim.32
  206.2 7.5 %all-to-all-start.9 = ((f32[64,1,256]{2,1,0:T(1,128)}), f32[64,1,256]{2,1,0:T(1,128)S(1)}, u32[]{:S(2)}, u32[]{:S(2)}) async-start(f32[64,1,256]{2,1,0:T(1,128)} %broadcast_in_dim.32), calls=%async_computation.9 | async-start | bytes 131072 | tf_op jit(solution)/shard_map/all_to_all | solution.py:15
  213.7 1.1 fusion.22
  214.8 10.0 %all-to-all-done.9 = f32[64,1,256]{2,1,0:T(1,128)S(1)} async-done(((f32[64,1,256]{2,1,0:T(1,128)}), f32[64,1,256]{2,1,0:T(1,128)S(1)}, u32[]{:S(2)}, u32[]{:S(2)}) %all-to-all-start.9) | async-done | bytes 65568 | tf_op jit(solution)/shard_map/all_to_all | solution.py:15
  224.7 1.0 broadcast_in_dim.30
  225.7 3.5 %all-to-all-start.6 = ((bf16[8,24,2048]{2,1,0:T(8,128)(2,1)}), bf16[8,24,2048]{2,1,0:T(8,128)(2,1)S(1)}, u32[]{:S(2)}, u32[]{:S(2)}) async-start(bf16[8,24,2048]{2,1,0:T(8,128)(2,1)} %broadcast_in_dim.30), calls=%async_computation.6 | async-start | bytes 1572864 | tf_op jit(solution)/shard_map/all_to_all | solution.py:15
  229.3 0.7 reduce_sum.82
  229.9 0.0 copy-done.7
  229.9 20.1 %all-to-all-done.6 = bf16[8,24,2048]{2,1,0:T(8,128)(2,1)S(1)} async-done(((bf16[8,24,2048]{2,1,0:T(8,128)(2,1)}), bf16[8,24,2048]{2,1,0:T(8,128)(2,1)S(1)}, u32[]{:S(2)}, u32[]{:S(2)}) %all-to-all-start.6) | async-done | bytes 786464 | tf_op jit(solution)/shard_map/all_to_all | solution.py:15
  250.0 0.2 broadcast_in_dim.31
  250.2 7.9 %all_to_all.54 = bf16[2,192,2048]{2,1,0:T(8,128)(2,1)S(1)} all-to-all(bf16[2,192,2048]{2,1,0:T(8,128)(2,1)S(1)} %broadcast_in_dim.31), channel_id=1, replica_groups=mesh['z'=8,'y'=8,'x'=8,'c'=2] {'c'}, dimensions={0} | all-to-all | bytes 3145728 | tf_op jit(solution)/shard_map/all_to_all | solution.py:15
  258.1 1.1 copy.46
  (5 shorter events, 0.1 us)
Async XLA Ops:
  0.6 128.3 %copy-start = (bf16[384,2048]{1,0:T(8,128)(2,1)S(1)}, bf16[384,2048]{1,0:T(8,128)(2,1)}, u32[]{:S(2)}) copy-start(bf16[384,2048]{1,0:T(8,128)(2,1)} %param.11) | copy-start | bytes 4718596
  2.9 16.7 %all-to-all-start = ((bf16[8,32,384]{2,1,0:T(8,128)(2,1)}), bf16[8,32,384]{2,1,0:T(8,128)(2,1)S(1)}, u32[]{:S(2)}, u32[]{:S(2)}) async-start(bf16[8,32,384]{2,1,0:T(8,128)(2,1)} %broadcast_in_dim.26), calls=%async_computation | async-start | bytes 393216 | tf_op jit(solution)/shard_map/all_to_all | solution.py:15
  85.2 6.0 %copy-start.8 = (f32[2048]{0:T(1024)S(1)}, f32[2048]{0:T(1024)}, u32[]{:S(2)}) copy-start(f32[2048]{0:T(1024)} %param.7) | copy-start | bytes 24580
  85.2 41.3 %all-to-all-start.3 = ((bf16[8,8,32,384]{3,2,1,0:T(8,128)(2,1)}), bf16[8,8,32,384]{3,2,1,0:T(8,128)(2,1)S(1)}, u32[]{:S(2)}, u32[]{:S(2)}) async-start(bf16[8,8,32,384]{3,2,1,0:T(8,128)(2,1)} %broadcast_in_dim.29), calls=%async_computation.3 | async-start | bytes 3145728 | tf_op jit(solution)/shard_map/all_to_all | solution.py:15
  89.4 1.9 copy-start.1
  126.6 1.4 copy-start.3
  128.9 2.2 copy-start.5
  128.9 1.6 copy-start.2
  142.3 6.6 %copy-start.6 = (f32[384,256]{0,1:T(8,128)S(1)}, f32[384,256]{0,1:T(8,128)}, u32[]{:S(2)}) copy-start(f32[384,256]{0,1:T(8,128)} %copy-done.5) | copy-start | bytes 1179652
  142.3 30.2 %all-to-all-start.5 = ((bf16[8,24,2048]{2,1,0:T(8,128)(2,1)}), bf16[8,24,2048]{2,1,0:T(8,128)(2,1)S(1)}, u32[]{:S(2)}, u32[]{:S(2)}) async-start(bf16[8,24,2048]{2,1,0:T(8,128)(2,1)} %bitcast.28), calls=%async_computation.5 | async-start | bytes 1572864 | tf_op jit(solution)/shard_map/all_to_all | solution.py:15
  172.5 32.8 %all-to-all-start.8 = ((bf16[64,32,256]{2,1,0:T(8,128)(2,1)}), bf16[64,32,256]{2,1,0:T(8,128)(2,1)S(1)}, u32[]{:S(2)}, u32[]{:S(2)}) async-start(bf16[64,32,256]{2,1,0:T(8,128)(2,1)} %bitcast.12), calls=%async_computation.8 | async-start | bytes 2097152 | tf_op jit(solution)/shard_map/all_to_all | solution.py:15
  178.3 1.2 copy-start.4
  205.5 24.5 %copy-start.7 = (f32[32,256]{1,0:T(8,128)}, f32[32,256]{1,0:T(8,128)S(1)}, u32[]{:S(2)}) copy-start(f32[32,256]{1,0:T(8,128)S(1)} %convert_reduce_fusion) | copy-start | bytes 98308
  206.2 18.6 %all-to-all-start.9 = ((f32[64,1,256]{2,1,0:T(1,128)}), f32[64,1,256]{2,1,0:T(1,128)S(1)}, u32[]{:S(2)}, u32[]{:S(2)}) async-start(f32[64,1,256]{2,1,0:T(1,128)} %broadcast_in_dim.32), calls=%async_computation.9 | async-start | bytes 131072 | tf_op jit(solution)/shard_map/all_to_all | solution.py:15
  225.7 24.3 %all-to-all-start.6 = ((bf16[8,24,2048]{2,1,0:T(8,128)(2,1)}), bf16[8,24,2048]{2,1,0:T(8,128)(2,1)S(1)}, u32[]{:S(2)}, u32[]{:S(2)}) async-start(bf16[8,24,2048]{2,1,0:T(8,128)(2,1)} %broadcast_in_dim.30), calls=%async_computation.6 | async-start | bytes 1572864 | tf_op jit(solution)/shard_map/all_to_all | solution.py:15
